TPU v7x, 256 devices: a 4x2x16 block of a 4x16x16 slice. The times are simulated.
256 devices in a mesh: grp: 2 (over y), sp: 32 (over z, core), tp: 4 (over x).
Axes of the slice: x: 4, y: 2, z: 16, core: 2. Of those that a mesh axis runs over, the one named last changes fastest.
The devices are a block of a 4x16x16 slice.
Arguments:
- hidden_in: bfloat16 [16384, 2048], P(('grp', 'sp')), parts along dimension 0, may hold values from -6 to 6
- query_latent_rows: bfloat16 [16384, 768], P(('grp', 'sp')), parts along dimension 0, may hold values from -6 to 6
- key_value_latent: bfloat16 [16384, 512], P(('grp', 'sp')), parts along dimension 0, may hold values from -6 to 6
- rotary_key: bfloat16 [16384, 32], P(('grp', 'sp')), parts along dimension 0, may hold values from -64 to 64
- query_norm_gain: float32 [768], replicated, may hold values from 0.1 to 1.9
- key_value_gain: float32 [512], replicated, may hold values from 0.1 to 1.9
- query_up_weight: bfloat16 [768, 1536], P(None, 'tp'), may hold values from -0.625 to 0.625
- key_value_up_weight: bfloat16 [512, 2048], P(None, 'tp'), may hold values from -0.25 to 0.25
- out_proj: bfloat16 [1024, 2048], P('tp'), may hold values from -0.1875 to 0.1875
- feed_gain: float32 [2048], replicated, may hold values from 0.1 to 1.9
- feed_up: bfloat16 [2048, 8192], P('sp', 'tp'), may hold values from -0.125 to 0.125
- feed_down: bfloat16 [8192, 2048], P('tp', 'sp'), may hold values from -0.0625 to 0.0625
Outputs:
- layer_out: bfloat16 [16384, 2048], P(('grp', 'sp', 'tp')), parts along dimension 0
There are 2 independent parts, one for each index of `grp`. A program takes and returns all parts, laid end to end along the dimension named above; an argument that names none is the same for every part. Nothing has to cross between parts.
All inputs are finite; a program needn't handle non-finite values.
Results may differ from a plain program's by a relative error of at most 0.02.
Values may be sent and summed in bfloat16 or wider, within the bound.
No kernel may reach another device: no remote copies, remote signals or barrier semaphores. Data moves between devices by JAX's collectives and lax.ppermute only.
A program may use at most 128 MiB of HBM per device.

v0:
```python
import math

import jax
import jax.numpy as jnp
from jax import lax
from jax.sharding import PartitionSpec as P

QUERY_KEY_PLAIN = 64
QUERY_KEY_ROTARY = 32
VALUE_HEAD_SIZE = 64


def cut_along(value, dim, count):
    before, after = (value.shape[:dim], value.shape[dim + 1 :])
    return jnp.moveaxis(value.reshape(*before, count, -1, *after), dim, 0)


def sum_at_owner(value, axis, dim):
    count = lax.axis_size(axis)
    pieces = lax.all_to_all(cut_along(value, dim, count), axis, 0, 0, tiled=True)
    return jnp.sum(pieces.astype(jnp.float32), axis=0)


def from_everyone(value, axis):
    copies = jnp.broadcast_to(value, (lax.axis_size(axis), *value.shape))
    return lax.all_to_all(copies, axis, split_axis=0, concat_axis=0, tiled=True)


def in_order(pieces, dim):
    lengths = list(pieces.shape[1:])
    lengths[dim] *= pieces.shape[0]
    return jnp.moveaxis(pieces, 0, dim).reshape(lengths)


def gather_directly(value, axis, dim):
    pieces = from_everyone(value, axis)
    return in_order(pieces, dim)


def normalize(values, gain):
    floats = values.astype(jnp.float32)
    return floats * lax.rsqrt(jnp.mean(floats * floats, axis=-1, keepdims=True) + 1e-06) * gain


def rotate(values, position):
    half_size = values.shape[-1] // 2
    inverse = 10000.0 ** (-jnp.arange(half_size, dtype=jnp.float32) * 2.0 / values.shape[-1])
    angles = position[:, None] * inverse[None, :]
    cosine = jnp.concatenate([jnp.cos(angles), jnp.cos(angles)], axis=-1)
    sine = jnp.concatenate([jnp.sin(angles), jnp.sin(angles)], axis=-1)
    shape = (values.shape[0],) + (1,) * (values.ndim - 2) + (values.shape[-1],)
    turned = jnp.concatenate([-values[..., half_size:], values[..., :half_size]], axis=-1)
    return values * cosine.reshape(shape) + turned * sine.reshape(shape)


def on_device(
    hidden_in,
    query_latent_rows,
    key_value_latent,
    rotary_key,
    query_norm_gain,
    key_value_gain,
    query_up_weight,
    key_value_up_weight,
    out_proj,
    feed_gain,
    feed_up,
    feed_down,
):
    tokens_here = hidden_in.shape[0]
    heads_here = query_up_weight.shape[1] // (QUERY_KEY_PLAIN + QUERY_KEY_ROTARY)
    position = (lax.axis_index("sp") * tokens_here + jnp.arange(tokens_here)).astype(jnp.float32)
    scale_factor = (QUERY_KEY_PLAIN + QUERY_KEY_ROTARY) ** (-0.5)
    query_norm = normalize(query_latent_rows, query_norm_gain).astype(jnp.bfloat16)
    queries = jnp.dot(query_norm, query_up_weight, preferred_element_type=jnp.float32).reshape(
        tokens_here, heads_here, QUERY_KEY_PLAIN + QUERY_KEY_ROTARY
    )
    queries = jnp.concatenate(
        [queries[..., :QUERY_KEY_PLAIN], rotate(queries[..., QUERY_KEY_PLAIN:], position)], axis=-1
    ).astype(jnp.bfloat16)
    query_plain = queries[..., :QUERY_KEY_PLAIN]
    query_turned = queries[..., QUERY_KEY_PLAIN:]
    latent = normalize(key_value_latent, key_value_gain).astype(jnp.bfloat16)
    key_rope = rotate(rotary_key.astype(jnp.float32), position).astype(jnp.bfloat16)

    def attend_block(carry, key_plain, value_rows, rope_rows):
        row_max, denom, accum = carry
        scores = jnp.einsum(
            "qhd,khd->hqk", query_plain, key_plain, preferred_element_type=jnp.float32
        )
        scores = scores + jnp.einsum(
            "qhd,kd->hqk", query_turned, rope_rows, preferred_element_type=jnp.float32
        )
        scores = scores * scale_factor
        new_max = jnp.maximum(row_max, jnp.max(scores, axis=-1))
        expo = jnp.exp(scores - new_max[:, :, None])
        factor = jnp.exp(row_max - new_max)
        denom = denom * factor + jnp.sum(expo, axis=-1)
        update = jnp.einsum(
            "hqk,khd->qhd",
            expo.astype(jnp.bfloat16),
            value_rows,
            preferred_element_type=jnp.float32,
        )
        accum = accum * jnp.transpose(factor)[:, :, None] + update
        return (new_max, denom, accum)

    start_carry = (
        jnp.full((heads_here, tokens_here), -1e30, jnp.float32),
        jnp.zeros((heads_here, tokens_here), jnp.float32),
        jnp.zeros((tokens_here, heads_here, VALUE_HEAD_SIZE), jnp.float32),
    )
    own_keys = jnp.dot(latent, key_value_up_weight, preferred_element_type=jnp.float32).astype(
        jnp.bfloat16
    )
    pieces = (
        lax.all_gather(own_keys, "sp", axis=0, tiled=True),
        lax.all_gather(key_rope, "sp", axis=0, tiled=True),
    )
    rows_in = pieces[0].shape[0]
    block = math.gcd(rows_in, 1024)

    def step_block(index, inner):
        first = index * block
        bulk = lax.dynamic_slice_in_dim(pieces[0], first, block, 0)
        rope_rows = lax.dynamic_slice_in_dim(pieces[1], first, block, 0)
        bulk = bulk.reshape(block, heads_here, QUERY_KEY_PLAIN + VALUE_HEAD_SIZE)
        return attend_block(
            inner, bulk[..., :QUERY_KEY_PLAIN], bulk[..., QUERY_KEY_PLAIN:], rope_rows
        )

    final_carry = lax.fori_loop(0, rows_in // block, step_block, start_carry)
    denom = final_carry[1]
    accum = final_carry[2]
    mixed = (
        (accum / jnp.transpose(denom)[:, :, None])
        .astype(jnp.bfloat16)
        .reshape(tokens_here, heads_here * VALUE_HEAD_SIZE)
    )
    share = tokens_here // lax.axis_size("tp")
    lead = lax.axis_index("tp") * share
    branch = sum_at_owner(
        jnp.dot(mixed, out_proj, preferred_element_type=jnp.float32).astype(jnp.bfloat16), "tp", 0
    )
    own_rows = lax.dynamic_slice_in_dim(hidden_in, lead, share, 0)
    middle_own = (own_rows.astype(jnp.float32) + branch).astype(jnp.bfloat16)
    normed = gather_directly(normalize(middle_own, feed_gain).astype(jnp.bfloat16), "tp", 0)
    upward = jnp.dot(
        normed,
        lax.all_gather(feed_up, "sp", axis=0, tiled=True),
        preferred_element_type=jnp.float32,
    )
    activated = jnp.square(jax.nn.relu(upward)).astype(jnp.bfloat16)
    partial_sum = jnp.dot(
        activated,
        lax.all_gather(feed_down, "sp", axis=1, tiled=True),
        preferred_element_type=jnp.float32,
    )
    feed = sum_at_owner(partial_sum.astype(jnp.bfloat16), "tp", 0)
    return (middle_own.astype(jnp.float32) + feed).astype(jnp.bfloat16)


def solution(mesh):
    return jax.shard_map(
        on_device,
        mesh=mesh,
        in_specs=(
            P(("grp", "sp"), None),
            P(("grp", "sp"), None),
            P(("grp", "sp"), None),
            P(("grp", "sp"), None),
            P(),
            P(),
            P(None, "tp"),
            P(None, "tp"),
            P("tp", None),
            P(),
            P("sp", "tp"),
            P("tp", "sp"),
        ),
        out_specs=P(("grp", "sp", "tp"), None),
        check_vma=False,
    )
```

profile of v0, /device:TPU:33, one launch (start us, length us, event | category | flops | bytes accessed | tf_op | source)
XLA Modules:
  0.0 289.8 jit_solution(13299205808065012109)
XLA Ops:
  7.7 2.2 convolution_convert_fusion.2
  14.2 1.6 fusion.32
  16.1 55.3 %all_gather.13 = bf16[8192,32]{0,1:T(8,128)(2,1)} all-gather(bf16[256,32]{0,1:T(8,128)(2,1)S(1)} %get-tuple-element.215), channel_id=1, replica_groups=mesh['grp'=2,'sp'=32,'tp'=4] {'sp'}, dimensions={0}, use_global_device_ids=true | all-gather | bytes 540672 | tf_op jit(solution)/shard_map/all_gather | solution.py:118
  72.0 30.9 %all-gather.4.cloned.1.call-done = bf16[8192,512]{1,0:T(8,128)(2,1)} async-done(((bf16[256,512]{1,0:T(8,128)(2,1)}), bf16[8192,512]{1,0:T(8,128)(2,1)}) %all-gather.4.cloned.1.call-update) | async-done | bytes 8388624 | tf_op jit(solution)/shard_map/all_gather | solution.py:117
  102.9 83.0 %while.18 = (s32[]{:T(128)}, f32[4,256]{1,0:T(4,128)S(1)}, f32[4,256]{1,0:T(4,128)S(1)}, f32[256,4,64]{0,2,1:T(8,128)S(1)}, bf16[8192,512]{1,0:T(8,128)(2,1)}, /...) while((s32[]{:T(128)}, f32[4,256]{1,0:T(4,128)S(1)}, ...), condition=%wide.region_5.0_spmd.clone, body=%wide.region_2.0_spmd.clone.sunk | while | flops 343087104 | bytes 44105964 | solution.py:132
  105.6 3.5 %fusion.71 = (f32[4,256]{1,0:T(4,128)S(1)}, f32[4,256,1024]{1,2,0:T(8,128)}) fusion(bf16[256,4,32]{0,2,1:T(8,128)(2,1)S(1)} %copy-done.2, bf16[8192,32]{0,1:T(8,128)(2,1)} %get-tuple-element.307, s32[]{:T(128)S(6)} %select_n.14, f32[4,1024,256]{2,1,0:T(8,128)S(1)} %fusion.70), kind=kOutput, calls=%fused_computation.74.clone.1 | convolution fusion | flops 70253568 | bytes 8523780 | tf_op jit(solution)/shard_map/while/body/eval_jaxpr/qhd,kd->hqk/dot_general | solution.py:91
  109.1 3.1 %fusion.75 = f32[256,4,64]{0,2,1:T(8,128)S(1)} fusion(f32[4,256,1024]{1,2,0:T(8,128)} %get-tuple-element.275, f32[4,256]{1,0:T(4,128)S(1)} %get-tuple-element.302, bf16[1024,4,128]{0,2,1:T(8,128)(2,1)S(1)} %bitcast.46, f32[256,4,64]{0,2,1:T(8,128)S(1)} %get-tuple-element.292, f32[256,4]{0,1:T(4,128)S(1)} %get-tuple-element.276, pred[]{:T(512)S(6)} %compare.3), kind=kOutput, calls=%fused_computation.8.clone.1 | convolution fusion | flops 136511488 | bytes 5251073 | tf_op jit(solution)/shard_map/while/body/eval_jaxpr/hqk,khd->qhd/dot_general | solution.py:99
  113.2 1.3 constant_dynamic-slice_fusion.2
  115.9 3.5 %fusion.71 = (f32[4,256]{1,0:T(4,128)S(1)}, f32[4,256,1024]{1,2,0:T(8,128)}) fusion(bf16[256,4,32]{0,2,1:T(8,128)(2,1)S(1)} %copy-done.2, bf16[8192,32]{0,1:T(8,128)(2,1)} %get-tuple-element.307, s32[]{:T(128)S(6)} %select_n.14, f32[4,1024,256]{2,1,0:T(8,128)S(1)} %fusion.70), kind=kOutput, calls=%fused_computation.74.clone.1 | convolution fusion | flops 70253568 | bytes 8523780 | tf_op jit(solution)/shard_map/while/body/eval_jaxpr/qhd,kd->hqk/dot_general | solution.py:91
  119.4 3.2 %fusion.75 = f32[256,4,64]{0,2,1:T(8,128)S(1)} fusion(f32[4,256,1024]{1,2,0:T(8,128)} %get-tuple-element.275, f32[4,256]{1,0:T(4,128)S(1)} %get-tuple-element.302, bf16[1024,4,128]{0,2,1:T(8,128)(2,1)S(1)} %bitcast.46, f32[256,4,64]{0,2,1:T(8,128)S(1)} %get-tuple-element.292, f32[256,4]{0,1:T(4,128)S(1)} %get-tuple-element.276, pred[]{:T(512)S(6)} %compare.3), kind=kOutput, calls=%fused_computation.8.clone.1 | convolution fusion | flops 136511488 | bytes 5251073 | tf_op jit(solution)/shard_map/while/body/eval_jaxpr/hqk,khd->qhd/dot_general | solution.py:99
  123.6 1.3 constant_dynamic-slice_fusion.2
  126.3 3.5 %fusion.71 = (f32[4,256]{1,0:T(4,128)S(1)}, f32[4,256,1024]{1,2,0:T(8,128)}) fusion(bf16[256,4,32]{0,2,1:T(8,128)(2,1)S(1)} %copy-done.2, bf16[8192,32]{0,1:T(8,128)(2,1)} %get-tuple-element.307, s32[]{:T(128)S(6)} %select_n.14, f32[4,1024,256]{2,1,0:T(8,128)S(1)} %fusion.70), kind=kOutput, calls=%fused_computation.74.clone.1 | convolution fusion | flops 70253568 | bytes 8523780 | tf_op jit(solution)/shard_map/while/body/eval_jaxpr/qhd,kd->hqk/dot_general | solution.py:91
  129.8 3.2 %fusion.75 = f32[256,4,64]{0,2,1:T(8,128)S(1)} fusion(f32[4,256,1024]{1,2,0:T(8,128)} %get-tuple-element.275, f32[4,256]{1,0:T(4,128)S(1)} %get-tuple-element.302, bf16[1024,4,128]{0,2,1:T(8,128)(2,1)S(1)} %bitcast.46, f32[256,4,64]{0,2,1:T(8,128)S(1)} %get-tuple-element.292, f32[256,4]{0,1:T(4,128)S(1)} %get-tuple-element.276, pred[]{:T(512)S(6)} %compare.3), kind=kOutput, calls=%fused_computation.8.clone.1 | convolution fusion | flops 136511488 | bytes 5251073 | tf_op jit(solution)/shard_map/while/body/eval_jaxpr/hqk,khd->qhd/dot_general | solution.py:99
  136.7 3.5 %fusion.71 = (f32[4,256]{1,0:T(4,128)S(1)}, f32[4,256,1024]{1,2,0:T(8,128)}) fusion(bf16[256,4,32]{0,2,1:T(8,128)(2,1)S(1)} %copy-done.2, bf16[8192,32]{0,1:T(8,128)(2,1)} %get-tuple-element.307, s32[]{:T(128)S(6)} %select_n.14, f32[4,1024,256]{2,1,0:T(8,128)S(1)} %fusion.70), kind=kOutput, calls=%fused_computation.74.clone.1 | convolution fusion | flops 70253568 | bytes 8523780 | tf_op jit(solution)/shard_map/while/body/eval_jaxpr/qhd,kd->hqk/dot_general | solution.py:91
  140.3 3.2 %fusion.75 = f32[256,4,64]{0,2,1:T(8,128)S(1)} fusion(f32[4,256,1024]{1,2,0:T(8,128)} %get-tuple-element.275, f32[4,256]{1,0:T(4,128)S(1)} %get-tuple-element.302, bf16[1024,4,128]{0,2,1:T(8,128)(2,1)S(1)} %bitcast.46, f32[256,4,64]{0,2,1:T(8,128)S(1)} %get-tuple-element.292, f32[256,4]{0,1:T(4,128)S(1)} %get-tuple-element.276, pred[]{:T(512)S(6)} %compare.3), kind=kOutput, calls=%fused_computation.8.clone.1 | convolution fusion | flops 136511488 | bytes 5251073 | tf_op jit(solution)/shard_map/while/body/eval_jaxpr/hqk,khd->qhd/dot_general | solution.py:99
  144.5 1.3 constant_dynamic-slice_fusion.2
  147.2 3.5 %fusion.71 = (f32[4,256]{1,0:T(4,128)S(1)}, f32[4,256,1024]{1,2,0:T(8,128)}) fusion(bf16[256,4,32]{0,2,1:T(8,128)(2,1)S(1)} %copy-done.2, bf16[8192,32]{0,1:T(8,128)(2,1)} %get-tuple-element.307, s32[]{:T(128)S(6)} %select_n.14, f32[4,1024,256]{2,1,0:T(8,128)S(1)} %fusion.70), kind=kOutput, calls=%fused_computation.74.clone.1 | convolution fusion | flops 70253568 | bytes 8523780 | tf_op jit(solution)/shard_map/while/body/eval_jaxpr/qhd,kd->hqk/dot_general | solution.py:91
  150.7 3.2 %fusion.75 = f32[256,4,64]{0,2,1:T(8,128)S(1)} fusion(f32[4,256,1024]{1,2,0:T(8,128)} %get-tuple-element.275, f32[4,256]{1,0:T(4,128)S(1)} %get-tuple-element.302, bf16[1024,4,128]{0,2,1:T(8,128)(2,1)S(1)} %bitcast.46, f32[256,4,64]{0,2,1:T(8,128)S(1)} %get-tuple-element.292, f32[256,4]{0,1:T(4,128)S(1)} %get-tuple-element.276, pred[]{:T(512)S(6)} %compare.3), kind=kOutput, calls=%fused_computation.8.clone.1 | convolution fusion | flops 136511488 | bytes 5251073 | tf_op jit(solution)/shard_map/while/body/eval_jaxpr/hqk,khd->qhd/dot_general | solution.py:99
  154.9 1.3 constant_dynamic-slice_fusion.2
  157.6 3.5 %fusion.71 = (f32[4,256]{1,0:T(4,128)S(1)}, f32[4,256,1024]{1,2,0:T(8,128)}) fusion(bf16[256,4,32]{0,2,1:T(8,128)(2,1)S(1)} %copy-done.2, bf16[8192,32]{0,1:T(8,128)(2,1)} %get-tuple-element.307, s32[]{:T(128)S(6)} %select_n.14, f32[4,1024,256]{2,1,0:T(8,128)S(1)} %fusion.70), kind=kOutput, calls=%fused_computation.74.clone.1 | convolution fusion | flops 70253568 | bytes 8523780 | tf_op jit(solution)/shard_map/while/body/eval_jaxpr/qhd,kd->hqk/dot_general | solution.py:91
  161.2 3.2 %fusion.75 = f32[256,4,64]{0,2,1:T(8,128)S(1)} fusion(f32[4,256,1024]{1,2,0:T(8,128)} %get-tuple-element.275, f32[4,256]{1,0:T(4,128)S(1)} %get-tuple-element.302, bf16[1024,4,128]{0,2,1:T(8,128)(2,1)S(1)} %bitcast.46, f32[256,4,64]{0,2,1:T(8,128)S(1)} %get-tuple-element.292, f32[256,4]{0,1:T(4,128)S(1)} %get-tuple-element.276, pred[]{:T(512)S(6)} %compare.3), kind=kOutput, calls=%fused_computation.8.clone.1 | convolution fusion | flops 136511488 | bytes 5251073 | tf_op jit(solution)/shard_map/while/body/eval_jaxpr/hqk,khd->qhd/dot_general | solution.py:99
  168.0 3.5 %fusion.71 = (f32[4,256]{1,0:T(4,128)S(1)}, f32[4,256,1024]{1,2,0:T(8,128)}) fusion(bf16[256,4,32]{0,2,1:T(8,128)(2,1)S(1)} %copy-done.2, bf16[8192,32]{0,1:T(8,128)(2,1)} %get-tuple-element.307, s32[]{:T(128)S(6)} %select_n.14, f32[4,1024,256]{2,1,0:T(8,128)S(1)} %fusion.70), kind=kOutput, calls=%fused_computation.74.clone.1 | convolution fusion | flops 70253568 | bytes 8523780 | tf_op jit(solution)/shard_map/while/body/eval_jaxpr/qhd,kd->hqk/dot_general | solution.py:91
  171.6 3.1 %fusion.75 = f32[256,4,64]{0,2,1:T(8,128)S(1)} fusion(f32[4,256,1024]{1,2,0:T(8,128)} %get-tuple-element.275, f32[4,256]{1,0:T(4,128)S(1)} %get-tuple-element.302, bf16[1024,4,128]{0,2,1:T(8,128)(2,1)S(1)} %bitcast.46, f32[256,4,64]{0,2,1:T(8,128)S(1)} %get-tuple-element.292, f32[256,4]{0,1:T(4,128)S(1)} %get-tuple-element.276, pred[]{:T(512)S(6)} %compare.3), kind=kOutput, calls=%fused_computation.8.clone.1 | convolution fusion | flops 136511488 | bytes 5251073 | tf_op jit(solution)/shard_map/while/body/eval_jaxpr/hqk,khd->qhd/dot_general | solution.py:99
  178.3 3.5 %fusion.71 = (f32[4,256]{1,0:T(4,128)S(1)}, f32[4,256,1024]{1,2,0:T(8,128)}) fusion(bf16[256,4,32]{0,2,1:T(8,128)(2,1)S(1)} %copy-done.2, bf16[8192,32]{0,1:T(8,128)(2,1)} %get-tuple-element.307, s32[]{:T(128)S(6)} %select_n.14, f32[4,1024,256]{2,1,0:T(8,128)S(1)} %fusion.70), kind=kOutput, calls=%fused_computation.74.clone.1 | convolution fusion | flops 70253568 | bytes 8523780 | tf_op jit(solution)/shard_map/while/body/eval_jaxpr/qhd,kd->hqk/dot_general | solution.py:91
  181.8 3.1 %fusion.75 = f32[256,4,64]{0,2,1:T(8,128)S(1)} fusion(f32[4,256,1024]{1,2,0:T(8,128)} %get-tuple-element.275, f32[4,256]{1,0:T(4,128)S(1)} %get-tuple-element.302, bf16[1024,4,128]{0,2,1:T(8,128)(2,1)S(1)} %bitcast.46, f32[256,4,64]{0,2,1:T(8,128)S(1)} %get-tuple-element.292, f32[256,4]{0,1:T(4,128)S(1)} %get-tuple-element.276, pred[]{:T(512)S(6)} %compare.3), kind=kOutput, calls=%fused_computation.8.clone.1 | convolution fusion | flops 136511488 | bytes 5251073 | tf_op jit(solution)/shard_map/while/body/eval_jaxpr/hqk,khd->qhd/dot_general | solution.py:99
  185.9 1.4 convolution_convert_fusion
  187.4 4.2 %all-to-all-start = ((bf16[4,64,2048]{2,1,0:T(8,128)(2,1)}), bf16[4,64,2048]{2,1,0:T(8,128)(2,1)S(1)}, u32[]{:S(2)}, u32[]{:S(2)}) async-start(bf16[4,64,2048]{2,1,0:T(8,128)(2,1)} %bitcast.3), calls=%async_computation | async-start | bytes 2097152 | tf_op jit(solution)/shard_map/all_to_all | solution.py:20
  191.5 14.8 %all-to-all-done = bf16[4,64,2048]{2,1,0:T(8,128)(2,1)S(1)} async-done(((bf16[4,64,2048]{2,1,0:T(8,128)(2,1)}), bf16[4,64,2048]{2,1,0:T(8,128)(2,1)S(1)}, u32[]{:S(2)}, u32[]{:S(2)}) %all-to-all-start) | async-done | bytes 1048608 | tf_op jit(solution)/shard_map/all_to_all | solution.py:20
  208.9 3.6 %all-to-all-start.1 = ((bf16[4,64,2048]{2,1,0:T(8,128)(2,1)}), bf16[4,64,2048]{2,1,0:T(8,128)(2,1)S(1)}, u32[]{:S(2)}, u32[]{:S(2)}) async-start(bf16[4,64,2048]{2,1,0:T(8,128)(2,1)} %broadcast_in_dim.17), calls=%async_computation.1 | async-start | bytes 2097152 | tf_op jit(solution)/shard_map/all_to_all | solution.py:26
  212.5 41.0 %all-gather.8.cloned.1.call-done = bf16[2048,2048]{0,1:T(8,128)(2,1)} async-done(((bf16[2048,64]{0,1:T(8,128)(2,1)}), bf16[2048,2048]{0,1:T(8,128)(2,1)}) %all-gather.8.cloned.1.call-update) | async-done | bytes 8388624 | tf_op jit(solution)/shard_map/all_gather | solution.py:156
  253.6 10.3 %convolution_convert_fusion.1 = bf16[256,2048]{1,0:T(8,128)(2,1)S(1)} fusion(bf16[2048,2048]{0,1:T(8,128)(2,1)} %all-gather.8.cloned.1.call-done, bf16[256,2048]{1,0:T(8,128)(2,1)S(1)} %bitcast.50, bf16[2048,2048]{1,0:T(8,128)(2,1)} %all-gather.6.cloned.1.call-done), kind=kOutput, calls=%fused_computation.26 | convolution fusion | flops 4297064448 | bytes 18874368 | tf_op jit(solution)/shard_map/dot_general | solution.py:154
  263.8 18.5 %all_to_all.15 = bf16[4,64,2048]{2,1,0:T(8,128)(2,1)S(1)} all-to-all(bf16[4,64,2048]{2,1,0:T(8,128)(2,1)S(1)} %bitcast.51), channel_id=1, replica_groups=mesh['grp'=2,'sp'=32,'tp'=4] {'tp'}, dimensions={0} | all-to-all | bytes 2097152 | tf_op jit(solution)/shard_map/all_to_all | solution.py:20
  (122 shorter events, 33.4 us)
Async XLA Ops:
  6.5 179.4 %copy-start = (bf16[256,2048]{1,0:T(8,128)(2,1)S(1)}, bf16[256,2048]{1,0:T(8,128)(2,1)}, u32[]{:S(2)}) copy-start(bf16[256,2048]{1,0:T(8,128)(2,1)} %param.22) | copy-start | bytes 3145732
  6.6 9.5 %copy-start.3 = (bf16[256,32]{0,1:T(8,128)(2,1)S(1)}, bf16[256,32]{0,1:T(8,128)(2,1)}, u32[]{:S(2)}) copy-start(bf16[256,32]{0,1:T(8,128)(2,1)} %param.17) | copy-start | bytes 49156
  6.6 96.4 %all-gather.4.cloned.1.call-start = ((), (), s32[]{:S(2)}) async-start(), calls=%async_computation.3 | async-start | bytes 8650752 | tf_op jit(solution)/shard_map/all_gather | solution.py:117
  10.0 202.5 %all-gather.6.cloned.1.call-start = ((), (), s32[]{:S(2)}) async-start(), calls=%async_computation.4 | async-start | bytes 8650752 | tf_op jit(solution)/shard_map/all_gather | solution.py:150
  10.8 242.7 %all-gather.8.cloned.1.call-start = ((), (), s32[]{:S(2)}) async-start(), calls=%async_computation.5 | async-start | bytes 8650752 | tf_op jit(solution)/shard_map/all_gather | solution.py:156
  104.8 0.8 copy-start.2
  109.1 3.4 %copy-start.1 = (f32[4,256,1024]{1,2,0:T(8,128)S(1)}, f32[4,256,1024]{1,2,0:T(8,128)}, u32[]{:S(2)}) copy-start(f32[4,256,1024]{1,2,0:T(8,128)} %get-tuple-element.275) | copy-start | bytes 12582916 | tf_op jit(solution)/shard_map/while
  115.0 0.8 copy-start.2
  119.4 3.6 %copy-start.1 = (f32[4,256,1024]{1,2,0:T(8,128)S(1)}, f32[4,256,1024]{1,2,0:T(8,128)}, u32[]{:S(2)}) copy-start(f32[4,256,1024]{1,2,0:T(8,128)} %get-tuple-element.275) | copy-start | bytes 12582916 | tf_op jit(solution)/shard_map/while
  125.5 0.8 copy-start.2
  129.8 3.6 %copy-start.1 = (f32[4,256,1024]{1,2,0:T(8,128)S(1)}, f32[4,256,1024]{1,2,0:T(8,128)}, u32[]{:S(2)}) copy-start(f32[4,256,1024]{1,2,0:T(8,128)} %get-tuple-element.275) | copy-start | bytes 12582916 | tf_op jit(solution)/shard_map/while
  135.9 0.8 copy-start.2
  140.3 3.6 %copy-start.1 = (f32[4,256,1024]{1,2,0:T(8,128)S(1)}, f32[4,256,1024]{1,2,0:T(8,128)}, u32[]{:S(2)}) copy-start(f32[4,256,1024]{1,2,0:T(8,128)} %get-tuple-element.275) | copy-start | bytes 12582916 | tf_op jit(solution)/shard_map/while
  146.3 0.8 copy-start.2
  150.7 3.6 %copy-start.1 = (f32[4,256,1024]{1,2,0:T(8,128)S(1)}, f32[4,256,1024]{1,2,0:T(8,128)}, u32[]{:S(2)}) copy-start(f32[4,256,1024]{1,2,0:T(8,128)} %get-tuple-element.275) | copy-start | bytes 12582916 | tf_op jit(solution)/shard_map/while
  156.8 0.8 copy-start.2
  161.2 3.6 %copy-start.1 = (f32[4,256,1024]{1,2,0:T(8,128)S(1)}, f32[4,256,1024]{1,2,0:T(8,128)}, u32[]{:S(2)}) copy-start(f32[4,256,1024]{1,2,0:T(8,128)} %get-tuple-element.275) | copy-start | bytes 12582916 | tf_op jit(solution)/shard_map/while
  167.2 0.8 copy-start.2
  171.6 3.4 %copy-start.1 = (f32[4,256,1024]{1,2,0:T(8,128)S(1)}, f32[4,256,1024]{1,2,0:T(8,128)}, u32[]{:S(2)}) copy-start(f32[4,256,1024]{1,2,0:T(8,128)} %get-tuple-element.275) | copy-start | bytes 12582916 | tf_op jit(solution)/shard_map/while
  177.5 0.8 copy-start.2
  181.8 3.4 %copy-start.1 = (f32[4,256,1024]{1,2,0:T(8,128)S(1)}, f32[4,256,1024]{1,2,0:T(8,128)}, u32[]{:S(2)}) copy-start(f32[4,256,1024]{1,2,0:T(8,128)} %get-tuple-element.275) | copy-start | bytes 12582916 | tf_op jit(solution)/shard_map/while
  185.9 21.7 %copy-start.4 = (f32[2048]{0:T(1024)S(1)}, f32[2048]{0:T(1024)}, u32[]{:S(2)}) copy-start(f32[2048]{0:T(1024)} %param.23) | copy-start | bytes 24580
  187.4 18.9 %all-to-all-start = ((bf16[4,64,2048]{2,1,0:T(8,128)(2,1)}), bf16[4,64,2048]{2,1,0:T(8,128)(2,1)S(1)}, u32[]{:S(2)}, u32[]{:S(2)}) async-start(bf16[4,64,2048]{2,1,0:T(8,128)(2,1)} %bitcast.3), calls=%async_computation | async-start | bytes 2097152 | tf_op jit(solution)/shard_map/all_to_all | solution.py:20
  208.9 44.7 %all-to-all-start.1 = ((bf16[4,64,2048]{2,1,0:T(8,128)(2,1)}), bf16[4,64,2048]{2,1,0:T(8,128)(2,1)S(1)}, u32[]{:S(2)}, u32[]{:S(2)}) async-start(bf16[4,64,2048]{2,1,0:T(8,128)(2,1)} %broadcast_in_dim.17), calls=%async_computation.1 | async-start | bytes 2097152 | tf_op jit(solution)/shard_map/all_to_all | solution.py:26
Sparse Core Ops, SparseCore 0:
  10.1 92.7 all-gather.3
  104.8 73.3 all-gather.5
  180.1 73.4 all-gather.7
where the time goes:
time: 291 us; the launch traced here: 290 us
  waiting for transfers between devices  88.2 us (30%)
  matrix products  75.2 us (26%)
  blocking collectives  73.7 us (25%)
  local copies, waits for them, and re-layouts  19.8 us (7%)
  between operations  13.3 us (5%)
  other arithmetic  11.1 us (4%)
  starting transfers between devices  7.9 us (3%)
    all_gather x1, blocking collectives, on_device(): lax.all_gather(key_rope, 'sp', axis=0, tiled=True)  55.3 us
    all_gather x1, waiting for transfers between devices, on_device(): lax.all_gather(feed_down, 'sp', axis=1, tiled=True)  41 us
    all_gather x1, waiting for transfers between devices, on_device(): lax.all_gather(own_keys, 'sp', axis=0, tiled=True)  30.9 us
    dot_general x8, matrix products, attend_block(): jnp.einsum('qhd,kd->hqk', query_turned, rope_rows, preferred_element_type...  28.1 us
    dot_general x8, matrix products, attend_block(): jnp.einsum('hqk,khd->qhd', expo.astype(jnp.bfloat16), value_rows, preferr...  25.4 us
    all_to_all x1, blocking collectives, sum_at_owner(): lax.all_to_all(cut_along(value, dim, count), axis, 0, 0, tiled=True)  18.5 us
    all_to_all x1, waiting for transfers between devices, sum_at_owner(): lax.all_to_all(cut_along(value, dim, count), axis, 0, 0, tiled=True)  14.8 us
    dynamic_slice x16, local copies, waits for them, and re-layouts, step_block(): bulk = lax.dynamic_slice_in_dim(pieces[0], first, block, 0)  14.7 us
  transfers between devices with their start and end apart: 5, of which 3 were waited for; matrix products, arithmetic and copies ran while one was open for 30% of the time, Pallas kernels for 0%

commit v1 on v0

v1 whole, which is shorter than its diff:
```python
import math

import jax
import jax.numpy as jnp
from jax import lax
from jax.experimental import pallas as pl
from jax.experimental.pallas import tpu as pltpu
from jax.sharding import PartitionSpec as P

PLAIN = 64
ROTARY = 32
VALUE = 64
CORES = 2
EPS = 1e-06


def normalize(values, gain):
    floats = values.astype(jnp.float32)
    return floats * lax.rsqrt(jnp.mean(floats * floats, axis=-1, keepdims=True) + EPS) * gain


def kv_body(latent_ref, gain_ref, weight_ref, rope_ref, cos_ref, sin_ref, out_ref):
    tokens = latent_ref.shape[0]
    half = ROTARY // 2
    latent = normalize(latent_ref[...], gain_ref[...]).astype(jnp.bfloat16)
    out_ref[:tokens, :] = jnp.dot(
        latent, weight_ref[...], preferred_element_type=jnp.float32
    ).astype(jnp.bfloat16)
    first, second = rope_ref[:half, :], rope_ref[half:, :]
    cos, sin = cos_ref[...], sin_ref[...]
    turned = jnp.concatenate([first * cos - second * sin, second * cos + first * sin], axis=1)
    out_ref[tokens:, :] = turned.astype(jnp.bfloat16)


def query_body(latent_ref, gain_ref, weight_ref, cos_ref, sin_ref, out_ref):
    half = ROTARY // 2
    size = PLAIN + ROTARY
    query_norm = normalize(latent_ref[...], gain_ref[...]).astype(jnp.bfloat16)
    queries = jnp.dot(query_norm, weight_ref[...], preferred_element_type=jnp.float32).T
    factor = size ** (-0.5) * math.log2(math.e)
    cos, sin = cos_ref[...], sin_ref[...]
    for head in range(queries.shape[0] // size):
        at = head * size
        first = queries[at + PLAIN : at + PLAIN + half]
        second = queries[at + PLAIN + half : at + size]
        rows = jnp.concatenate(
            [queries[at : at + PLAIN], first * cos - second * sin, second * cos + first * sin],
            axis=0,
        )
        out_ref[at : at + size, :] = (rows * factor).astype(jnp.bfloat16)


def attend_body(count, begins, *refs):
    pieces, query_ref = refs[:count], refs[count]
    state_ref = None if begins else refs[count + 1]
    out_ref = refs[-1]
    heads = query_ref.shape[0]
    tokens = pieces[0].shape[0] - ROTARY // 2
    ropes, turned_values = [], []
    for piece in pieces:
        low = piece[tokens:, :]
        rope = jnp.concatenate([low[:, :tokens], low[:, tokens:]], axis=0).astype(jnp.float32)
        rope = jnp.concatenate([rope, jnp.zeros((128 - ROTARY, tokens), jnp.float32)], axis=0)
        ropes.append(rope.T.astype(jnp.bfloat16))
        turned_values.append(piece[:tokens, :].T)
    ones = jnp.ones((16, tokens), jnp.bfloat16)
    for head in range(heads):
        at = head * (PLAIN + VALUE)
        scores = []
        for piece, rope in zip(pieces, ropes):
            left = jnp.concatenate([piece[:tokens, at : at + PLAIN + VALUE], rope], axis=1)
            scores.append(
                jnp.dot(left, query_ref[head], preferred_element_type=jnp.float32)
            )
        top = jnp.max(scores[0], axis=0, keepdims=True)
        for one in scores[1:]:
            top = jnp.maximum(top, jnp.max(one, axis=0, keepdims=True))
        if begins:
            total = None
        else:
            before = state_ref[head, VALUE + 8 : VALUE + 9, :]
            top = jnp.maximum(top, before)
            total = state_ref[head, : VALUE + 16, :] * jnp.exp2(before - top)
        for one, values in zip(scores, turned_values):
            weights = jnp.exp2(one - top).astype(jnp.bfloat16)
            left = jnp.concatenate([values[at + PLAIN : at + PLAIN + VALUE], ones], axis=0)
            update = jnp.dot(left, weights, preferred_element_type=jnp.float32)
            total = update if total is None else total + update
        out_ref[head, : VALUE + 8, :] = total[: VALUE + 8]
        out_ref[head, VALUE + 8 :, :] = jnp.broadcast_to(top, (8, top.shape[1]))


def attend(pieces, queries, state):
    heads, _, columns = queries.shape
    begins = state is None
    operands = (*pieces, queries) + (() if begins else (state,))
    keys = sum(piece.shape[0] - ROTARY // 2 for piece in pieces)
    return pl.pallas_call(
        lambda *refs: attend_body(len(pieces), begins, *refs),
        out_shape=jax.ShapeDtypeStruct((heads, VALUE + 16, columns), jnp.float32),
        cost_estimate=pl.CostEstimate(
            flops=2 * heads * keys * columns * (256 + 128),
            bytes_accessed=2 * keys * 512,
            transcendentals=heads * keys * columns,
        ),
        name="attend",
    )(*operands)


def feed_body(normed_ref, weight_ref, out_ref, sum_ref, act_ref):
    step = pl.program_id(0)
    half = pl.num_programs(0) // 2
    blocks, _, rows, width = weight_ref.shape
    weight = weight_ref[...].reshape(blocks * rows, width)

    @pl.when(step < half)
    def _():
        part = jnp.dot(normed_ref[...], weight, preferred_element_type=jnp.float32)

        @pl.when(step == 0)
        def _():
            sum_ref[...] = part

        @pl.when(jnp.logical_and(step > 0, step < half - 1))
        def _():
            sum_ref[...] += part

        @pl.when(step == half - 1)
        def _():
            act_ref[...] = jnp.square(jnp.maximum(sum_ref[...] + part, 0.0)).astype(jnp.bfloat16)

    @pl.when(step >= half)
    def _():
        out_ref[...] = lax.dot_general(
            act_ref[...], weight, (((1,), (1,)), ((), ())), preferred_element_type=jnp.float32
        ).astype(jnp.bfloat16)


def feed(normed, gathered, shares):
    tokens, width = normed.shape
    hidden = gathered.shape[1]
    rows = gathered.shape[0] // (2 * shares)
    stacked = gathered.reshape(shares, 2, rows, hidden)
    half = 4
    group = shares // half
    return pl.pallas_call(
        feed_body,
        grid=(2 * half,),
        in_specs=[
            pl.BlockSpec((tokens, group * rows), lambda i: (0, jnp.minimum(i, half - 1))),
            pl.BlockSpec((group, 1, rows, hidden), lambda i: (i % half, i // half, 0, 0)),
        ],
        out_specs=pl.BlockSpec((tokens, group * rows), lambda i: (0, jnp.maximum(i - half, 0))),
        out_shape=jax.ShapeDtypeStruct((tokens, width), jnp.bfloat16),
        scratch_shapes=[
            pltpu.VMEM((tokens, hidden), jnp.float32),
            pltpu.VMEM((tokens, hidden), jnp.bfloat16),
        ],
        cost_estimate=pl.CostEstimate(
            flops=4 * tokens * width * hidden,
            bytes_accessed=4 * width * hidden,
            transcendentals=0,
        ),
        name="feed",
    )(normed, stacked)


def swap_sum(value, axis):
    count = lax.axis_size(axis)
    pieces = lax.all_to_all(
        value.reshape(count, -1, value.shape[-1]), axis, 0, 0, tiled=True
    )
    return jnp.sum(pieces.astype(jnp.float32), axis=0)


def from_everyone(value, axis):
    copies = jnp.broadcast_to(value, (lax.axis_size(axis), *value.shape))
    return lax.all_to_all(copies, axis, split_axis=0, concat_axis=0, tiled=True)


def on_device(
    hidden_in,
    query_latent_rows,
    key_value_latent,
    rotary_key,
    query_norm_gain,
    key_value_gain,
    query_up_weight,
    key_value_up_weight,
    out_proj,
    feed_gain,
    feed_up,
    feed_down,
):
    tokens = hidden_in.shape[0]
    shares = lax.axis_size("sp")
    heads = query_up_weight.shape[1] // (PLAIN + ROTARY)
    kv_width = key_value_up_weight.shape[1]
    half = ROTARY // 2

    weights = lax.all_gather(
        jnp.concatenate([feed_up, feed_down.T], axis=0), "sp", axis=0, tiled=True
    )

    position = (lax.axis_index("sp") * tokens + jnp.arange(tokens)).astype(jnp.float32)
    inverse = 10000.0 ** (-jnp.arange(half, dtype=jnp.float32) * 2.0 / ROTARY)
    angles = inverse[:, None] * position[None, :]
    cos, sin = jnp.cos(angles), jnp.sin(angles)

    own = pl.pallas_call(
        kv_body,
        out_shape=jax.ShapeDtypeStruct((tokens + half, kv_width), jnp.bfloat16),
        name="keys_values",
    )(
        key_value_latent,
        key_value_gain.reshape(1, -1),
        key_value_up_weight,
        rotary_key.astype(jnp.float32).T,
        cos,
        sin,
    )
    query_rows = pl.pallas_call(
        query_body,
        out_shape=jax.ShapeDtypeStruct((heads * (PLAIN + ROTARY), tokens), jnp.bfloat16),
        name="queries",
    )(query_latent_rows, query_norm_gain.reshape(1, -1), query_up_weight, cos, sin)

    partner = [(i, i ^ 1) for i in range(shares)]
    upward = [(i, (i + CORES) % shares) for i in range(shares)]
    downward = [(j, i) for i, j in upward]
    other_rows = lax.ppermute(query_rows, "sp", partner)
    both = jnp.concatenate([query_rows, other_rows], axis=1).reshape(
        heads, PLAIN + ROTARY, 2 * tokens
    )
    columns = 2 * tokens
    queries = jnp.concatenate(
        [
            both[:, :PLAIN],
            jnp.zeros((heads, VALUE, columns), jnp.bfloat16),
            both[:, PLAIN:],
            jnp.zeros((heads, 128 - ROTARY, columns), jnp.bfloat16),
        ],
        axis=1,
    )

    ring = shares // CORES
    up, down = own, own
    pieces = [own]
    state = None
    for step in range(ring // 2 + 1):
        with jax.named_scope(f"ring_{step}"):
            arriving = []
            if step < ring // 2:
                up = lax.ppermute(up, "sp", upward)
                arriving.append(up)
            if step < (ring - 1) // 2:
                down = lax.ppermute(down, "sp", downward)
                arriving.append(down)
            state = attend(pieces, queries, state)
            pieces = arriving

    theirs = lax.ppermute(state[:, :, tokens:], "sp", partner)
    mine = state[:, :, :tokens]
    at_top = VALUE + 8
    top = jnp.maximum(mine[:, at_top : at_top + 1], theirs[:, at_top : at_top + 1])
    mine = mine[:, : VALUE + 1] * jnp.exp2(mine[:, at_top : at_top + 1] - top)
    theirs = theirs[:, : VALUE + 1] * jnp.exp2(theirs[:, at_top : at_top + 1] - top)
    summed = mine + theirs
    mixed = (summed[:, :VALUE] / summed[:, VALUE:]).astype(jnp.bfloat16)
    mixed = mixed.reshape(heads * VALUE, tokens)

    share = tokens // lax.axis_size("tp")
    lead = lax.axis_index("tp") * share
    branch = swap_sum(
        lax.dot_general(
            mixed, out_proj, (((0,), (0,)), ((), ())), preferred_element_type=jnp.float32
        ).astype(jnp.bfloat16),
        "tp",
    )
    own_rows = lax.dynamic_slice_in_dim(hidden_in, lead, share, 0)
    middle = (own_rows.astype(jnp.float32) + branch).astype(jnp.bfloat16)
    normed = from_everyone(normalize(middle, feed_gain).astype(jnp.bfloat16), "tp")
    normed = normed.reshape(tokens, -1)
    result = swap_sum(feed(normed, weights, shares), "tp")
    return (middle.astype(jnp.float32) + result).astype(jnp.bfloat16)


def solution(mesh):
    return jax.shard_map(
        on_device,
        mesh=mesh,
        in_specs=(
            P(("grp", "sp"), None),
            P(("grp", "sp"), None),
            P(("grp", "sp"), None),
            P(("grp", "sp"), None),
            P(),
            P(),
            P(None, "tp"),
            P(None, "tp"),
            P("tp", None),
            P(),
            P("sp", "tp"),
            P("tp", "sp"),
        ),
        out_specs=P(("grp", "sp", "tp"), None),
        check_vma=False,
    )
```

time: 291 us -> 252 us (0.87)
  matrix products: 75.2 us -> 1.45 us
  Pallas kernels: 0 us -> 57.4 us
  starting transfers between devices: 7.9 us -> 56.4 us
  blocking collectives: 73.7 us -> 32.7 us
  local copies, waits for them, and re-layouts: 19.8 us -> 3.39 us
  waiting for transfers between devices: 88.2 us -> 72.7 us
    dot_general x28 -> x1, matrix products: 75.2 us -> 1.45 us  [on_device(): lax.dot_general(mixed, out_proj, (((0,), (0,)), ((), ())), preferred_elem...]
    all_gather x3 -> x1, waiting for transfers between devices: 71.9 us -> 0.01 us  [on_device(): lax.all_gather(jnp.concatenate([feed_up, feed_down.T], axis=0), 'sp', axi...]
    ppermute x0 -> x17, waiting for transfers between devices: none -> 58.1 us  [the longest x8 47.7 us: on_device(): up = lax.ppermute(up, 'sp', upward)]
    pallas_call x0 -> x12, Pallas kernels: none -> 57.4 us  [the longest x9 40 us: attend(): pl.pallas_call(lambda *refs: attend_body(len(pieces), begins, *refs), out...]
    all_gather x1 -> x0, blocking collectives: 55.3 us -> none  [on_device(): lax.all_gather(key_rope, 'sp', axis=0, tiled=True)]
    ppermute x0 -> x17, starting transfers between devices: none -> 52 us  [the longest x7 39.1 us: on_device(): down = lax.ppermute(down, 'sp', downward)]
    dynamic_slice x16 -> x0, local copies, waits for them, and re-layouts: 14.7 us -> none  [step_block(): bulk = lax.dynamic_slice_in_dim(pieces[0], first, block, 0)]
    all_to_all x1 -> x2, blocking collectives: 18.5 us -> 32.7 us  [the longest x1 16.6 us: from_everyone(): return lax.all_to_all(copies, axis, split_axis=0, concat_axis=0, tiled=True)]
  transfers between devices with their start and end apart: 5 -> 19, of which waited for: 3 -> 12; matrix products, arithmetic and copies ran while one was open for 30% -> 4% of each run, Pallas kernels for 0% -> 18%
where the time goes in v1:
time: 252 us; the launch traced here: 248 us
  waiting for transfers between devices  72.7 us (29%)
  Pallas kernels  57.4 us (23%)
  starting transfers between devices  56.4 us (22%)
  blocking collectives  32.7 us (13%)
  between operations  13.6 us (5%)
  other arithmetic  10.4 us (4%)
  local copies, waits for them, and re-layouts  3.39 us (1%)
    ppermute x8, waiting for transfers between devices, on_device(): up = lax.ppermute(up, 'sp', upward)  47.7 us
    pallas_call x9, Pallas kernels, attend(): pl.pallas_call(lambda *refs: attend_body(len(pieces), begins, *refs), out...  40 us
    ppermute x7, starting transfers between devices, on_device(): down = lax.ppermute(down, 'sp', downward)  39.1 us
    all_to_all x1, blocking collectives, from_everyone(): return lax.all_to_all(copies, axis, split_axis=0, concat_axis=0, tiled=True)  16.6 us
    all_to_all x1, blocking collectives, swap_sum(): lax.all_to_all(value.reshape(count, -1, value.shape[-1]), axis, 0, 0, til...  16.1 us
    all_to_all x1, waiting for transfers between devices, swap_sum(): lax.all_to_all(value.reshape(count, -1, value.shape[-1]), axis, 0, 0, til...  14.5 us
    pallas_call x1, Pallas kernels, feed(): pl.pallas_call(feed_body, grid=(2 * half,), in_specs=[pl.BlockSpec((token...  12.7 us
    ppermute x7, waiting for transfers between devices, on_device(): down = lax.ppermute(down, 'sp', downward)  9.12 us
  transfers between devices with their start and end apart: 19, of which 12 were waited for; matrix products, arithmetic and copies ran while one was open for 4% of the time, Pallas kernels for 18%

profile of v1, /device:TPU:33, one launch (start us, length us, event | category | flops | bytes accessed | tf_op | source)
XLA Modules:
  0.0 248.0 jit_solution(1696640347886137577)
XLA Ops:
  13.0 3.3 %collective-permute-start = (bf16[272,512]{1,0:T(8,128)(2,1)}, bf16[272,512]{1,0:T(8,128)(2,1)S(1)}, u32[]{:S(2)}, u32[]{:S(2)}) collective-permute-start(bf16[272,512]{1,0:T(8,128)(2,1)} %keys_values.1.refs_0_), channel_id=1, source_target_pairs={{0,8},{4,12},{8,16},{12,20},{16,24},{20,28},{24,32},{28,36},{32,40... | collective-permute-start | bytes 835592 | tf_op jit(solution)/shard_map/ring_0/ppermute | solution.py:254
  16.3 19.6 %collective-permute-start.9 = (bf16[272,512]{1,0:T(8,128)(2,1)}, bf16[272,512]{1,0:T(8,128)(2,1)S(1)}, u32[]{:S(2)}, u32[]{:S(2)}) collective-permute-start(bf16[272,512]{1,0:T(8,128)(2,1)} %keys_values.1.refs_0_), channel_id=1, source_target_pairs={{8,0},{12,4},{16,8},{20,12},{24,16},{28,20},{32,24},{36,28},{40,32... | collective-permute-start | bytes 835592 | tf_op jit(solution)/shard_map/ring_0/ppermute | solution.py:257
  35.9 6.6 %collective-permute-done.refs_0_ = bf16[272,512]{1,0:T(8,128)(2,1)S(1)} collective-permute-done((bf16[272,512]{1,0:T(8,128)(2,1)}, bf16[272,512]{1,0:T(8,128)(2,1)S(1)}, u32[]{:S(2)}, u32[]{:S(2)}) %collective-permute-start) | collective-permute-done | bytes 278560 | tf_op jit(solution)/shard_map/ring_0/ppermute | solution.py:254
  44.1 3.4 %collective-permute-start.10 = (bf16[272,512]{1,0:T(8,128)(2,1)S(1)}, bf16[272,512]{1,0:T(8,128)(2,1)S(1)}, u32[]{:S(2)}, u32[]{:S(2)}) collective-permute-start(bf16[272,512]{1,0:T(8,128)(2,1)S(1)} %collective-permute-done.9.refs_1_), channel_id=1, source_target_pairs={{8,0},{12,4},{16,8},{20,12},{24,16},{28,20},{32,24},{36,28},{40,32... | collective-permute-start | bytes 835592 | tf_op jit(solution)/shard_map/ring_1/ppermute | solution.py:257
  47.6 10.3 %collective-permute-done.1.refs_0_ = bf16[272,512]{1,0:T(8,128)(2,1)S(1)} collective-permute-done((bf16[272,512]{1,0:T(8,128)(2,1)S(1)}, bf16[272,512]{1,0:T(8,128)(2,1)S(1)}, u32[]{:S(2)}, u32[]{:S(2)}) %collective-permute-start.1) | collective-permute-done | bytes 278560 | tf_op jit(solution)/shard_map/ring_1/ppermute | solution.py:254
  58.8 3.5 %collective-permute-start.11 = (bf16[272,512]{1,0:T(8,128)(2,1)S(1)}, bf16[272,512]{1,0:T(8,128)(2,1)S(1)}, u32[]{:S(2)}, u32[]{:S(2)}) collective-permute-start(bf16[272,512]{1,0:T(8,128)(2,1)S(1)} %collective-permute-done.10.refs_1_), channel_id=1, source_target_pairs={{8,0},{12,4},{16,8},{20,12},{24,16},{28,20},{32,24},{36,28},{40,32... | collective-permute-start | bytes 835592 | tf_op jit(solution)/shard_map/ring_2/ppermute | solution.py:257
  62.4 10.7 %collective-permute-done.2.refs_0_ = bf16[272,512]{1,0:T(8,128)(2,1)S(1)} collective-permute-done((bf16[272,512]{1,0:T(8,128)(2,1)S(1)}, bf16[272,512]{1,0:T(8,128)(2,1)S(1)}, u32[]{:S(2)}, u32[]{:S(2)}) %collective-permute-start.2) | collective-permute-done | bytes 278560 | tf_op jit(solution)/shard_map/ring_2/ppermute | solution.py:254
  73.5 3.5 %collective-permute-start.12 = (bf16[272,512]{1,0:T(8,128)(2,1)S(1)}, bf16[272,512]{1,0:T(8,128)(2,1)S(1)}, u32[]{:S(2)}, u32[]{:S(2)}) collective-permute-start(bf16[272,512]{1,0:T(8,128)(2,1)S(1)} %collective-permute-done.11.refs_1_), channel_id=1, source_target_pairs={{8,0},{12,4},{16,8},{20,12},{24,16},{28,20},{32,24},{36,28},{40,32... | collective-permute-start | bytes 835592 | tf_op jit(solution)/shard_map/ring_3/ppermute | solution.py:257
  77.0 11.1 %collective-permute-done.3.refs_0_ = bf16[272,512]{1,0:T(8,128)(2,1)S(1)} collective-permute-done((bf16[272,512]{1,0:T(8,128)(2,1)S(1)}, bf16[272,512]{1,0:T(8,128)(2,1)S(1)}, u32[]{:S(2)}, u32[]{:S(2)}) %collective-permute-start.3) | collective-permute-done | bytes 278560 | tf_op jit(solution)/shard_map/ring_3/ppermute | solution.py:254
  88.7 2.5 queries.1
  91.1 3.6 %collective-permute-start.8 = (bf16[384,256]{1,0:T(8,128)(2,1)}, bf16[384,256]{1,0:T(8,128)(2,1)S(1)}, u32[]{:S(2)}, u32[]{:S(2)}) collective-permute-start(bf16[384,256]{1,0:T(8,128)(2,1)} %queries.1), channel_id=1, source_target_pairs={{0,4},{4,0},{8,12},{12,8},{16,20},{20,16},{24,28},{28,24},{32,36},... | collective-permute-start | bytes 589832 | tf_op jit(solution)/shard_map/ppermute | solution.py:231
  94.8 2.9 %collective-permute-start.13 = (bf16[272,512]{1,0:T(8,128)(2,1)S(1)}, bf16[272,512]{1,0:T(8,128)(2,1)}, u32[]{:S(2)}, u32[]{:S(2)}) collective-permute-start(bf16[272,512]{1,0:T(8,128)(2,1)S(1)} %collective-permute-done.12.refs_1_), channel_id=1, source_target_pairs={{8,0},{12,4},{16,8},{20,12},{24,16},{28,20},{32,24},{36,28},{40,32... | collective-permute-start | bytes 835592 | tf_op jit(solution)/shard_map/ring_4/ppermute | solution.py:257
  97.7 5.1 %collective-permute-done.4.refs_0_ = bf16[272,512]{1,0:T(8,128)(2,1)} collective-permute-done((bf16[272,512]{1,0:T(8,128)(2,1)S(1)}, bf16[272,512]{1,0:T(8,128)(2,1)}, u32[]{:S(2)}, u32[]{:S(2)}) %collective-permute-start.4) | collective-permute-done | bytes 278560 | tf_op jit(solution)/shard_map/ring_4/ppermute | solution.py:254
  104.0 6.1 %collective-permute-done.13.refs_1_ = bf16[272,512]{1,0:T(8,128)(2,1)} collective-permute-done((bf16[272,512]{1,0:T(8,128)(2,1)S(1)}, bf16[272,512]{1,0:T(8,128)(2,1)}, u32[]{:S(2)}, u32[]{:S(2)}) %collective-permute-start.13) | collective-permute-done | bytes 278560 | tf_op jit(solution)/shard_map/ring_4/ppermute | solution.py:257
  110.1 3.5 %collective-permute-start.14 = (bf16[272,512]{1,0:T(8,128)(2,1)}, bf16[272,512]{1,0:T(8,128)(2,1)}, u32[]{:S(2)}, u32[]{:S(2)}) collective-permute-start(bf16[272,512]{1,0:T(8,128)(2,1)} %collective-permute-done.13.refs_1_), channel_id=1, source_target_pairs={{8,0},{12,4},{16,8},{20,12},{24,16},{28,20},{32,24},{36,28},{40,32... | collective-permute-start | bytes 835592 | tf_op jit(solution)/shard_map/ring_5/ppermute | solution.py:257
  113.6 3.9 %collective-permute-done.5.refs_0_ = bf16[272,512]{1,0:T(8,128)(2,1)} collective-permute-done((bf16[272,512]{1,0:T(8,128)(2,1)}, bf16[272,512]{1,0:T(8,128)(2,1)}, u32[]{:S(2)}, u32[]{:S(2)}) %collective-permute-start.5) | collective-permute-done | bytes 278560 | tf_op jit(solution)/shard_map/ring_5/ppermute | solution.py:254
  118.7 3.6 %attend.9.refs_3_ = f32[4,80,512]{2,1,0:T(8,128)} custom-call(bf16[272,512]{1,0:T(8,128)(2,1)} %keys_values.1.refs_0_, bf16[4,256,512]{2,1,0:T(8,128)(2,1)} %maximum_maximum_fusion.refs_1_.refs_2_), custom_call_target="tpu_custom_call" | custom-call | flops 402653184 | bytes 262144 | tf_op jit(solution)/shard_map/ring_0/attend/pallas_call | solution.py:98
  122.4 4.7 %attend.10.refs_3_ = f32[4,80,512]{2,1,0:T(8,128)} custom-call(bf16[272,512]{1,0:T(8,128)(2,1)} %copy-done.4, bf16[272,512]{1,0:T(8,128)(2,1)} %copy-done.5, bf16[4,256,512]{2,1,0:T(8,128)(2,1)} %maximum_maximum_fusion.refs_1_.refs_2_, f32[4,80,512]{2,1,0:T(8,128)} %attend.9.refs_3_), custom_call_target="tpu_custom_call" | custom-call | flops 805306368 | bytes 524288 | tf_op jit(solution)/shard_map/ring_1/attend/pallas_call | solution.py:98
  127.1 4.6 %attend.11.refs_3_ = f32[4,80,512]{2,1,0:T(8,128)} custom-call(bf16[272,512]{1,0:T(8,128)(2,1)} %copy-done.6, bf16[272,512]{1,0:T(8,128)(2,1)} %copy-done.8, bf16[4,256,512]{2,1,0:T(8,128)(2,1)} %maximum_maximum_fusion.refs_1_.refs_2_, f32[4,80,512]{2,1,0:T(8,128)} %attend.10.refs_3_), custom_call_target="tpu_custom_call" | custom-call | flops 805306368 | bytes 524288 | tf_op jit(solution)/shard_map/ring_2/attend/pallas_call | solution.py:98
  131.7 2.6 %collective-permute-start.15 = (bf16[272,512]{1,0:T(8,128)(2,1)}, bf16[272,512]{1,0:T(8,128)(2,1)S(1)}, u32[]{:S(2)}, u32[]{:S(2)}) collective-permute-start(bf16[272,512]{1,0:T(8,128)(2,1)} %collective-permute-done.14.refs_1_), channel_id=1, source_target_pairs={{8,0},{12,4},{16,8},{20,12},{24,16},{28,20},{32,24},{36,28},{40,32... | collective-permute-start | bytes 835592 | tf_op jit(solution)/shard_map/ring_6/ppermute | solution.py:257
  134.3 4.7 %attend.12.refs_3_ = f32[4,80,512]{2,1,0:T(8,128)} custom-call(bf16[272,512]{1,0:T(8,128)(2,1)} %copy-done.7, bf16[272,512]{1,0:T(8,128)(2,1)} %copy-done.10, bf16[4,256,512]{2,1,0:T(8,128)(2,1)} %maximum_maximum_fusion.refs_1_.refs_2_, f32[4,80,512]{2,1,0:T(8,128)} %attend.11.refs_3_), custom_call_target="tpu_custom_call" | custom-call | flops 805306368 | bytes 524288 | tf_op jit(solution)/shard_map/ring_3/attend/pallas_call | solution.py:98
  139.0 4.6 %attend.13.refs_3_ = f32[4,80,512]{2,1,0:T(8,128)} custom-call(bf16[272,512]{1,0:T(8,128)(2,1)} %copy-done.9, bf16[272,512]{1,0:T(8,128)(2,1)} %copy-done.11, bf16[4,256,512]{2,1,0:T(8,128)(2,1)} %maximum_maximum_fusion.refs_1_.refs_2_, f32[4,80,512]{2,1,0:T(8,128)} %attend.12.refs_3_), custom_call_target="tpu_custom_call" | custom-call | flops 805306368 | bytes 524288 | tf_op jit(solution)/shard_map/ring_4/attend/pallas_call | solution.py:98
  143.6 4.7 %attend.14.refs_3_ = f32[4,80,512]{2,1,0:T(8,128)} custom-call(bf16[272,512]{1,0:T(8,128)(2,1)} %collective-permute-done.4.refs_0_, bf16[272,512]{1,0:T(8,128)(2,1)} %collective-permute-done.13.refs_1_, bf16[4,256,512]{2,1,0:T(8,128)(2,1)} %maximum_maximum_fusion.refs_1_.refs_2_, f32[4,80,512]{2,1,0:T(8,128)} %attend.13.refs_3_), custom_call_target="tpu_custom_call" | custom-call | flops 805306368 | bytes 524288 | tf_op jit(solution)/shard_map/ring_5/attend/pallas_call | solution.py:98
  148.3 4.7 %attend.15.refs_3_ = f32[4,80,512]{2,1,0:T(8,128)} custom-call(bf16[272,512]{1,0:T(8,128)(2,1)} %collective-permute-done.5.refs_0_, bf16[272,512]{1,0:T(8,128)(2,1)} %collective-permute-done.14.refs_1_, bf16[4,256,512]{2,1,0:T(8,128)(2,1)} %maximum_maximum_fusion.refs_1_.refs_2_, f32[4,80,512]{2,1,0:T(8,128)} %attend.14.refs_3_), custom_call_target="tpu_custom_call" | custom-call | flops 805306368 | bytes 524288 | tf_op jit(solution)/shard_map/ring_6/attend/pallas_call | solution.py:98
  153.6 4.6 %attend.16.refs_2_ = f32[4,80,512]{2,1,0:T(8,128)} custom-call(bf16[272,512]{1,0:T(8,128)(2,1)} %collective-permute-done.6.refs_0_, bf16[272,512]{1,0:T(8,128)(2,1)} %copy-done.12, bf16[4,256,512]{2,1,0:T(8,128)(2,1)} %maximum_maximum_fusion.refs_1_.refs_2_, f32[4,80,512]{2,1,0:T(8,128)} %attend.15.refs_3_), custom_call_target="tpu_custom_call" | custom-call | flops 805306368 | bytes 524288 | tf_op jit(solution)/shard_map/ring_7/attend/pallas_call | solution.py:98
  159.0 3.8 %attend.17 = f32[4,80,512]{2,1,0:T(8,128)} custom-call(bf16[272,512]{1,0:T(8,128)(2,1)} %copy-done.1, bf16[4,256,512]{2,1,0:T(8,128)(2,1)} %maximum_maximum_fusion.refs_1_.refs_2_, f32[4,80,512]{2,1,0:T(8,128)} %attend.16.refs_2_), custom_call_target="tpu_custom_call" | custom-call | flops 402653184 | bytes 262144 | tf_op jit(solution)/shard_map/ring_8/attend/pallas_call | solution.py:98
  163.8 6.0 %collective-permute-start.16 = (f32[4,80,256]{2,1,0:T(8,128)S(1)}, f32[4,80,256]{2,1,0:T(8,128)S(1)}, u32[]{:S(2)}, u32[]{:S(2)}) collective-permute-start(f32[4,80,256]{2,1,0:T(8,128)S(1)} %slice.45), channel_id=1, source_target_pairs={{0,4},{4,0},{8,12},{12,8},{16,20},{20,16},{24,28},{28,24},{32,36},... | collective-permute-start | bytes 983048 | tf_op jit(solution)/shard_map/ppermute | solution.py:262
  174.3 4.4 %all-to-all-start = ((bf16[4,64,2048]{2,1,0:T(8,128)(2,1)}), bf16[4,64,2048]{2,1,0:T(8,128)(2,1)S(1)}, u32[]{:S(2)}, u32[]{:S(2)}) async-start(bf16[4,64,2048]{2,1,0:T(8,128)(2,1)} %bitcast.4), calls=%async_computation | async-start | bytes 2097152 | tf_op jit(solution)/shard_map/all_to_all | solution.py:170
  178.7 14.5 %all-to-all-done = bf16[4,64,2048]{2,1,0:T(8,128)(2,1)S(1)} async-done(((bf16[4,64,2048]{2,1,0:T(8,128)(2,1)}), bf16[4,64,2048]{2,1,0:T(8,128)(2,1)S(1)}, u32[]{:S(2)}, u32[]{:S(2)}) %all-to-all-start) | async-done | bytes 1048608 | tf_op jit(solution)/shard_map/all_to_all | solution.py:170
  194.8 16.6 %all_to_all.15 = bf16[4,64,2048]{2,1,0:T(8,128)(2,1)} all-to-all(bf16[4,64,2048]{2,1,0:T(8,128)(2,1)S(1)} %broadcast_in_dim.15), channel_id=1, replica_groups=mesh['grp'=2,'sp'=32,'tp'=4] {'tp'}, dimensions={0} | all-to-all | bytes 2097152 | tf_op jit(solution)/shard_map/all_to_all | solution.py:178
  211.4 12.7 %feed.1 = bf16[256,2048]{1,0:T(8,128)(2,1)} custom-call(bf16[256,2048]{1,0:T(8,128)(2,1)} %bitcast.20, bf16[32,2,64,2048]{3,2,1,0:T(8,128)(2,1)} %bitcast.19), custom_call_target="tpu_custom_call" | custom-call | flops 4294967296 | bytes 16777216 | tf_op jit(solution)/shard_map/feed/pallas_call | solution.py:146
  224.1 16.1 %all_to_all.16 = bf16[4,64,2048]{2,1,0:T(8,128)(2,1)S(1)} all-to-all(bf16[4,64,2048]{2,1,0:T(8,128)(2,1)} %bitcast.21), channel_id=1, replica_groups=mesh['grp'=2,'sp'=32,'tp'=4] {'tp'}, dimensions={0} | all-to-all | bytes 2097152 | tf_op jit(solution)/shard_map/all_to_all | solution.py:170
  (76 shorter events, 21.8 us)
Async XLA Ops:
  6.5 166.3 %copy-start = (bf16[256,2048]{1,0:T(8,128)(2,1)S(1)}, bf16[256,2048]{1,0:T(8,128)(2,1)}, u32[]{:S(2)}) copy-start(bf16[256,2048]{1,0:T(8,128)(2,1)} %param.20) | copy-start | bytes 3145732
  6.6 81.5 %copy-start.3 = (f32[768]{0:T(1024)S(1)}, f32[768]{0:T(1024)}, u32[]{:S(2)}) copy-start(f32[768]{0:T(1024)} %param.16) | copy-start | bytes 9220
  6.6 204.9 %all-gather.2.cloned.1.call-start = ((), (), s32[]{:S(2)}) async-start(), calls=%async_computation.3 | async-start | bytes 17301504 | tf_op jit(solution)/shard_map/all_gather | solution.py:201
  13.0 29.6 %collective-permute-start = (bf16[272,512]{1,0:T(8,128)(2,1)}, bf16[272,512]{1,0:T(8,128)(2,1)S(1)}, u32[]{:S(2)}, u32[]{:S(2)}) collective-permute-start(bf16[272,512]{1,0:T(8,128)(2,1)} %keys_values.1.refs_0_), channel_id=1, source_target_pairs={{0,8},{4,12},{8,16},{12,20},{16,24},{20,28},{24,32},{28,36},{32,40... | collective-permute-start | bytes 835592 | tf_op jit(solution)/shard_map/ring_0/ppermute | solution.py:254
  16.3 27.9 %collective-permute-start.9 = (bf16[272,512]{1,0:T(8,128)(2,1)}, bf16[272,512]{1,0:T(8,128)(2,1)S(1)}, u32[]{:S(2)}, u32[]{:S(2)}) collective-permute-start(bf16[272,512]{1,0:T(8,128)(2,1)} %keys_values.1.refs_0_), channel_id=1, source_target_pairs={{8,0},{12,4},{16,8},{20,12},{24,16},{28,20},{32,24},{36,28},{40,32... | collective-permute-start | bytes 835592 | tf_op jit(solution)/shard_map/ring_0/ppermute | solution.py:257
  42.5 76.2 %copy-start.4 = (bf16[272,512]{1,0:T(8,128)(2,1)}, bf16[272,512]{1,0:T(8,128)(2,1)S(1)}, u32[]{:S(2)}) copy-start(bf16[272,512]{1,0:T(8,128)(2,1)S(1)} %collective-permute-done.refs_0_) | copy-start | bytes 835588
  42.5 15.4 %collective-permute-start.1 = (bf16[272,512]{1,0:T(8,128)(2,1)S(1)}, bf16[272,512]{1,0:T(8,128)(2,1)S(1)}, u32[]{:S(2)}, u32[]{:S(2)}) collective-permute-start(bf16[272,512]{1,0:T(8,128)(2,1)S(1)} %collective-permute-done.refs_0_), channel_id=1, source_target_pairs={{0,8},{4,12},{8,16},{12,20},{16,24},{20,28},{24,32},{28,36},{32,40... | collective-permute-start | bytes 835592 | tf_op jit(solution)/shard_map/ring_1/ppermute | solution.py:254
  44.1 74.6 %copy-start.5 = (bf16[272,512]{1,0:T(8,128)(2,1)}, bf16[272,512]{1,0:T(8,128)(2,1)S(1)}, u32[]{:S(2)}) copy-start(bf16[272,512]{1,0:T(8,128)(2,1)S(1)} %collective-permute-done.9.refs_1_) | copy-start | bytes 835588
  44.1 14.7 %collective-permute-start.10 = (bf16[272,512]{1,0:T(8,128)(2,1)S(1)}, bf16[272,512]{1,0:T(8,128)(2,1)S(1)}, u32[]{:S(2)}, u32[]{:S(2)}) collective-permute-start(bf16[272,512]{1,0:T(8,128)(2,1)S(1)} %collective-permute-done.9.refs_1_), channel_id=1, source_target_pairs={{8,0},{12,4},{16,8},{20,12},{24,16},{28,20},{32,24},{36,28},{40,32... | collective-permute-start | bytes 835592 | tf_op jit(solution)/shard_map/ring_1/ppermute | solution.py:257
  57.9 60.8 %copy-start.6 = (bf16[272,512]{1,0:T(8,128)(2,1)}, bf16[272,512]{1,0:T(8,128)(2,1)S(1)}, u32[]{:S(2)}) copy-start(bf16[272,512]{1,0:T(8,128)(2,1)S(1)} %collective-permute-done.1.refs_0_) | copy-start | bytes 835588
  57.9 15.2 %collective-permute-start.2 = (bf16[272,512]{1,0:T(8,128)(2,1)S(1)}, bf16[272,512]{1,0:T(8,128)(2,1)S(1)}, u32[]{:S(2)}, u32[]{:S(2)}) collective-permute-start(bf16[272,512]{1,0:T(8,128)(2,1)S(1)} %collective-permute-done.1.refs_0_), channel_id=1, source_target_pairs={{0,8},{4,12},{8,16},{12,20},{16,24},{20,28},{24,32},{28,36},{32,40... | collective-permute-start | bytes 835592 | tf_op jit(solution)/shard_map/ring_2/ppermute | solution.py:254
  58.8 59.9 %copy-start.8 = (bf16[272,512]{1,0:T(8,128)(2,1)}, bf16[272,512]{1,0:T(8,128)(2,1)S(1)}, u32[]{:S(2)}) copy-start(bf16[272,512]{1,0:T(8,128)(2,1)S(1)} %collective-permute-done.10.refs_1_) | copy-start | bytes 835588
  58.8 14.6 %collective-permute-start.11 = (bf16[272,512]{1,0:T(8,128)(2,1)S(1)}, bf16[272,512]{1,0:T(8,128)(2,1)S(1)}, u32[]{:S(2)}, u32[]{:S(2)}) collective-permute-start(bf16[272,512]{1,0:T(8,128)(2,1)S(1)} %collective-permute-done.10.refs_1_), channel_id=1, source_target_pairs={{8,0},{12,4},{16,8},{20,12},{24,16},{28,20},{32,24},{36,28},{40,32... | collective-permute-start | bytes 835592 | tf_op jit(solution)/shard_map/ring_2/ppermute | solution.py:257
  73.1 45.7 %copy-start.7 = (bf16[272,512]{1,0:T(8,128)(2,1)}, bf16[272,512]{1,0:T(8,128)(2,1)S(1)}, u32[]{:S(2)}) copy-start(bf16[272,512]{1,0:T(8,128)(2,1)S(1)} %collective-permute-done.2.refs_0_) | copy-start | bytes 835588
  73.1 15.0 %collective-permute-start.3 = (bf16[272,512]{1,0:T(8,128)(2,1)S(1)}, bf16[272,512]{1,0:T(8,128)(2,1)S(1)}, u32[]{:S(2)}, u32[]{:S(2)}) collective-permute-start(bf16[272,512]{1,0:T(8,128)(2,1)S(1)} %collective-permute-done.2.refs_0_), channel_id=1, source_target_pairs={{0,8},{4,12},{8,16},{12,20},{16,24},{20,28},{24,32},{28,36},{32,40... | collective-permute-start | bytes 835592 | tf_op jit(solution)/shard_map/ring_3/ppermute | solution.py:254
  73.5 45.3 %copy-start.10 = (bf16[272,512]{1,0:T(8,128)(2,1)}, bf16[272,512]{1,0:T(8,128)(2,1)S(1)}, u32[]{:S(2)}) copy-start(bf16[272,512]{1,0:T(8,128)(2,1)S(1)} %collective-permute-done.11.refs_1_) | copy-start | bytes 835588
  73.5 21.3 %collective-permute-start.12 = (bf16[272,512]{1,0:T(8,128)(2,1)S(1)}, bf16[272,512]{1,0:T(8,128)(2,1)S(1)}, u32[]{:S(2)}, u32[]{:S(2)}) collective-permute-start(bf16[272,512]{1,0:T(8,128)(2,1)S(1)} %collective-permute-done.11.refs_1_), channel_id=1, source_target_pairs={{8,0},{12,4},{16,8},{20,12},{24,16},{28,20},{32,24},{36,28},{40,32... | collective-permute-start | bytes 835592 | tf_op jit(solution)/shard_map/ring_3/ppermute | solution.py:257
  88.0 30.7 %copy-start.9 = (bf16[272,512]{1,0:T(8,128)(2,1)}, bf16[272,512]{1,0:T(8,128)(2,1)S(1)}, u32[]{:S(2)}) copy-start(bf16[272,512]{1,0:T(8,128)(2,1)S(1)} %collective-permute-done.3.refs_0_) | copy-start | bytes 835588
  88.0 14.8 %collective-permute-start.4 = (bf16[272,512]{1,0:T(8,128)(2,1)S(1)}, bf16[272,512]{1,0:T(8,128)(2,1)}, u32[]{:S(2)}, u32[]{:S(2)}) collective-permute-start(bf16[272,512]{1,0:T(8,128)(2,1)S(1)} %collective-permute-done.3.refs_0_), channel_id=1, source_target_pairs={{0,8},{4,12},{8,16},{12,20},{16,24},{20,28},{24,32},{28,36},{32,40... | collective-permute-start | bytes 835592 | tf_op jit(solution)/shard_map/ring_4/ppermute | solution.py:254
  91.1 11.8 %collective-permute-start.8 = (bf16[384,256]{1,0:T(8,128)(2,1)}, bf16[384,256]{1,0:T(8,128)(2,1)S(1)}, u32[]{:S(2)}, u32[]{:S(2)}) collective-permute-start(bf16[384,256]{1,0:T(8,128)(2,1)} %queries.1), channel_id=1, source_target_pairs={{0,4},{4,0},{8,12},{12,8},{16,20},{20,16},{24,28},{28,24},{32,36},... | collective-permute-start | bytes 589832 | tf_op jit(solution)/shard_map/ppermute | solution.py:231
  94.8 27.6 %copy-start.11 = (bf16[272,512]{1,0:T(8,128)(2,1)}, bf16[272,512]{1,0:T(8,128)(2,1)S(1)}, u32[]{:S(2)}) copy-start(bf16[272,512]{1,0:T(8,128)(2,1)S(1)} %collective-permute-done.12.refs_1_) | copy-start | bytes 835588
  94.8 15.3 %collective-permute-start.13 = (bf16[272,512]{1,0:T(8,128)(2,1)S(1)}, bf16[272,512]{1,0:T(8,128)(2,1)}, u32[]{:S(2)}, u32[]{:S(2)}) collective-permute-start(bf16[272,512]{1,0:T(8,128)(2,1)S(1)} %collective-permute-done.12.refs_1_), channel_id=1, source_target_pairs={{8,0},{12,4},{16,8},{20,12},{24,16},{28,20},{32,24},{36,28},{40,32... | collective-permute-start | bytes 835592 | tf_op jit(solution)/shard_map/ring_4/ppermute | solution.py:257
  102.8 14.7 %collective-permute-start.5 = (bf16[272,512]{1,0:T(8,128)(2,1)}, bf16[272,512]{1,0:T(8,128)(2,1)}, u32[]{:S(2)}, u32[]{:S(2)}) collective-permute-start(bf16[272,512]{1,0:T(8,128)(2,1)} %collective-permute-done.4.refs_0_), channel_id=1, source_target_pairs={{0,8},{4,12},{8,16},{12,20},{16,24},{20,28},{24,32},{28,36},{32,40... | collective-permute-start | bytes 835592 | tf_op jit(solution)/shard_map/ring_5/ppermute | solution.py:254
  110.1 21.6 %collective-permute-start.14 = (bf16[272,512]{1,0:T(8,128)(2,1)}, bf16[272,512]{1,0:T(8,128)(2,1)}, u32[]{:S(2)}, u32[]{:S(2)}) collective-permute-start(bf16[272,512]{1,0:T(8,128)(2,1)} %collective-permute-done.13.refs_1_), channel_id=1, source_target_pairs={{8,0},{12,4},{16,8},{20,12},{24,16},{28,20},{32,24},{36,28},{40,32... | collective-permute-start | bytes 835592 | tf_op jit(solution)/shard_map/ring_5/ppermute | solution.py:257
  117.5 21.5 %collective-permute-start.6 = (bf16[272,512]{1,0:T(8,128)(2,1)}, bf16[272,512]{1,0:T(8,128)(2,1)}, u32[]{:S(2)}, u32[]{:S(2)}) collective-permute-start(bf16[272,512]{1,0:T(8,128)(2,1)} %collective-permute-done.5.refs_0_), channel_id=1, source_target_pairs={{0,8},{4,12},{8,16},{12,20},{16,24},{20,28},{24,32},{28,36},{32,40... | collective-permute-start | bytes 835592 | tf_op jit(solution)/shard_map/ring_6/ppermute | solution.py:254
  131.7 21.3 %collective-permute-start.15 = (bf16[272,512]{1,0:T(8,128)(2,1)}, bf16[272,512]{1,0:T(8,128)(2,1)S(1)}, u32[]{:S(2)}, u32[]{:S(2)}) collective-permute-start(bf16[272,512]{1,0:T(8,128)(2,1)} %collective-permute-done.14.refs_1_), channel_id=1, source_target_pairs={{8,0},{12,4},{16,8},{20,12},{24,16},{28,20},{32,24},{36,28},{40,32... | collective-permute-start | bytes 835592 | tf_op jit(solution)/shard_map/ring_6/ppermute | solution.py:257
  139.0 19.3 %collective-permute-start.7 = (bf16[272,512]{1,0:T(8,128)(2,1)}, bf16[272,512]{1,0:T(8,128)(2,1)S(1)}, u32[]{:S(2)}, u32[]{:S(2)}) collective-permute-start(bf16[272,512]{1,0:T(8,128)(2,1)} %collective-permute-done.6.refs_0_), channel_id=1, source_target_pairs={{0,8},{4,12},{8,16},{12,20},{16,24},{20,28},{24,32},{28,36},{32,40... | collective-permute-start | bytes 835592 | tf_op jit(solution)/shard_map/ring_7/ppermute | solution.py:254
  152.9 0.7 copy-start.12
  158.3 0.7 copy-start.1
  163.8 7.2 %collective-permute-start.16 = (f32[4,80,256]{2,1,0:T(8,128)S(1)}, f32[4,80,256]{2,1,0:T(8,128)S(1)}, u32[]{:S(2)}, u32[]{:S(2)}) collective-permute-start(f32[4,80,256]{2,1,0:T(8,128)S(1)} %slice.45), channel_id=1, source_target_pairs={{0,4},{4,0},{8,12},{12,8},{16,20},{20,16},{24,28},{28,24},{32,36},... | collective-permute-start | bytes 983048 | tf_op jit(solution)/shard_map/ppermute | solution.py:262
  174.3 20.2 %copy-start.2 = (f32[2048]{0:T(1024)S(1)}, f32[2048]{0:T(1024)}, u32[]{:S(2)}) copy-start(f32[2048]{0:T(1024)} %param.21) | copy-start | bytes 24580
  174.3 18.9 %all-to-all-start = ((bf16[4,64,2048]{2,1,0:T(8,128)(2,1)}), bf16[4,64,2048]{2,1,0:T(8,128)(2,1)S(1)}, u32[]{:S(2)}, u32[]{:S(2)}) async-start(bf16[4,64,2048]{2,1,0:T(8,128)(2,1)} %bitcast.4), calls=%async_computation | async-start | bytes 2097152 | tf_op jit(solution)/shard_map/all_to_all | solution.py:170
Sparse Core Ops, SparseCore 0:
  9.2 162.0 all-gather.1
